TPU v7x, 32 devices: a whole 2x2x4 slice. The times are simulated.
32 devices in a mesh: dp: 4 (over y, x), kv: 4 (over z), tp: 2 (over core).
Axes of the slice: x: 2, y: 2, z: 4, core: 2. Of those that a mesh axis runs over, the one named last changes fastest.
Arguments:
- tokens: bfloat16 [32, 4096], P('dp', ('kv', 'tp')), may hold values from -6 to 6
- w_query: bfloat16 [4096, 2, 1024], P(None, 'tp', 'kv'), may hold values from -0.09375 to 0.09375
- w_forget: bfloat16 [4096, 2, 1024], P(None, 'tp', 'kv'), may hold values from -0.09375 to 0.09375
- w_input: bfloat16 [4096, 2, 1024], P(None, 'tp', 'kv'), may hold values from -0.09375 to 0.09375
- w_output_gate: bfloat16 [4096, 2, 1024], P(None, 'tp', 'kv'), may hold values from -0.09375 to 0.09375
- gate_floor: float32 [2048], P('tp'), may hold values from 0 to 0.9
- head_gain: float32 [128], replicated, may hold values from 0.1 to 1.9
- w_out: bfloat16 [2048, 4096], P(None, ('kv', 'tp')), may hold values from -0.125 to 0.125
- mix_gain: float32 [4096], replicated, may hold values from 0.1 to 1.9
- ffn_gain: float32 [4096], replicated, may hold values from 0.1 to 1.9
- w_up: bfloat16 [4096, 16384], P(None, ('kv', 'tp')), may hold values from -0.09375 to 0.09375
- w_down: bfloat16 [16384, 4096], P(('kv', 'tp')), may hold values from -0.0625 to 0.0625
- state: float32 [32, 16, 128, 128], P(('dp', 'kv'), 'tp'), may hold values from -6 to 6
Outputs:
- mixed: bfloat16 [32, 4096], P('dp', ('kv', 'tp'))
- new_state: float32 [32, 16, 128, 128], P(('dp', 'kv'), 'tp')
All inputs are finite; a program needn't handle non-finite values.
Results may differ from a plain program's by a relative error of at most 0.014.
Values may be sent and summed in bfloat16 or wider, within the bound.
A program may use at most 128 MiB of HBM per device.

v0:
```python
import jax
import jax.numpy as jnp
from jax import lax
from jax.sharding import PartitionSpec as P

EPSILON = 1e-06


def rms_scale(values, gain):
    return values * lax.rsqrt(jnp.mean(values * values, axis=-1, keepdims=True) + EPSILON) * gain


def per_device(
    tokens,
    w_query,
    w_forget,
    w_input,
    w_output_gate,
    gate_floor,
    head_gain,
    w_out,
    mix_gain,
    ffn_gain,
    w_up,
    w_down,
    state,
):
    group_kv = lax.axis_size("kv")
    group_tp = lax.axis_size("tp")
    tokens_f = tokens.astype(jnp.float32)
    full_rows = lax.all_gather(tokens, ("kv", "tp"), axis=1, tiled=True)
    normed = rms_scale(full_rows.astype(jnp.float32), mix_gain).astype(jnp.bfloat16)

    def project(weight):
        return jnp.dot(normed, weight[:, 0, :], preferred_element_type=jnp.float32).astype(
            jnp.bfloat16
        )

    query_raw, forget_raw, input_raw, gate_raw = (
        lax.all_to_all(project(w_query), "kv", split_axis=0, concat_axis=1, tiled=True),
        lax.all_to_all(project(w_forget), "kv", split_axis=0, concat_axis=1, tiled=True),
        lax.all_to_all(project(w_input), "kv", split_axis=0, concat_axis=1, tiled=True),
        lax.all_to_all(project(w_output_gate), "kv", split_axis=0, concat_axis=1, tiled=True),
    )
    seq_local = state.shape[0]
    heads_local = state.shape[1]
    head_size = state.shape[2]
    query_vec = query_raw.astype(jnp.float32).reshape(
        seq_local, heads_local, head_size
    ) * head_size ** (-0.5)
    floor_heads = gate_floor.reshape(heads_local, head_size)
    forget_gate = floor_heads + (1.0 - floor_heads) * jax.nn.sigmoid(
        forget_raw.astype(jnp.float32).reshape(seq_local, heads_local, head_size)
    )
    input_vec = input_raw.astype(jnp.float32).reshape(seq_local, heads_local, head_size)
    gate_vec = gate_raw.astype(jnp.float32).reshape(seq_local, heads_local, head_size)
    new_state = (
        forget_gate[..., None] * state + (1.0 - forget_gate)[..., None] * input_vec[:, :, None, :]
    )
    head_out = jnp.einsum("bhk,bhkv->bhv", query_vec, new_state, precision=lax.Precision.HIGHEST)
    branch = rms_scale(head_out, head_gain) * jax.nn.silu(gate_vec)
    branch = branch.reshape(seq_local, 1, heads_local * head_size).astype(jnp.bfloat16)
    gathered = lax.all_gather(branch, ("kv", "tp"), axis=1, tiled=True)
    gathered = gathered.reshape(seq_local, group_kv, group_tp, heads_local * head_size)
    gathered = jnp.transpose(gathered, (1, 0, 2, 3)).reshape(
        group_kv * seq_local, group_tp * heads_local * head_size
    )
    projected = jnp.dot(gathered, w_out, preferred_element_type=jnp.float32)
    residual_one = (tokens_f + projected).astype(jnp.bfloat16)
    whole_rows = lax.all_gather(residual_one, ("kv", "tp"), axis=1, tiled=True)
    ffn_in = rms_scale(whole_rows.astype(jnp.float32), ffn_gain).astype(jnp.bfloat16)
    upward = jnp.dot(ffn_in, w_up, preferred_element_type=jnp.float32)
    hidden = jnp.square(jax.nn.relu(upward)).astype(jnp.bfloat16)
    partial_terms = jnp.dot(hidden, w_down, preferred_element_type=jnp.float32)
    summed = lax.psum_scatter(partial_terms, ("kv", "tp"), scatter_dimension=1, tiled=True)
    results = (residual_one.astype(jnp.float32) + summed).astype(jnp.bfloat16)
    return (results, new_state)


def solution(mesh):
    placed = (
        P("dp", ("kv", "tp")),
        P(None, "tp", "kv"),
        P(None, "tp", "kv"),
        P(None, "tp", "kv"),
        P(None, "tp", "kv"),
        P("tp"),
        P(),
        P(None, ("kv", "tp")),
        P(),
        P(),
        P(None, ("kv", "tp")),
        P(("kv", "tp"), None),
        P(("dp", "kv"), "tp", None, None),
    )
    return jax.shard_map(
        per_device,
        mesh=mesh,
        in_specs=placed,
        out_specs=(P("dp", ("kv", "tp")), P(("dp", "kv"), "tp", None, None)),
        check_vma=False,
    )
```

profile of v0, /device:TPU:0, one launch (start us, length us, event | category | flops | bytes accessed | tf_op | source)
XLA Modules:
  0.0 146.4 jit_solution(5957048308820464604)
XLA Ops:
  7.2 16.0 %all_gather.9 = bf16[8,4096]{1,0:T(8,128)(2,1)S(1)} all-gather(bf16[8,512]{1,0:T(8,128)(2,1)} %param.13), channel_id=1, replica_groups=mesh['dp'=4,'kv'=4,'tp'=2] {'kv','tp'}, dimensions={1}, use_global_device_ids=true | all-gather | bytes 73728 | tf_op jit(solution)/shard_map/all_gather | solution.py:31
  23.2 0.1 fusion.24
  23.4 2.0 %fusion.20 = bf16[8,256]{1,0:T(8,128)(2,1)S(1)} fusion(bf16[4096,1,256]{2,0,1:T(8,128)(2,1)} %param.17, bf16[8,4096]{1,0:T(8,128)(2,1)S(1)} %all_gather.9, f32[4096]{0:T(1024)} %param.21, f32[8]{0:T(128)S(1)} %add_rsqrt_fusion.2), kind=kOutput, calls=%fused_computation.16 | convolution fusion | flops 16910336 | bytes 2183200 | tf_op jit(solution)/shard_map/dot_general | solution.py:35
  25.4 0.6 all_to_all.46
  26.0 4.6 %all-to-all-start.3 = ((bf16[4,2,256]{2,1,0:T(2,128)(2,1)}), bf16[4,2,256]{2,1,0:T(2,128)(2,1)S(1)}, u32[]{:S(2)}, u32[]{:S(2)}) async-start(bf16[4,2,256]{2,1,0:T(2,128)(2,1)} %all_to_all.46), calls=%async_computation.3 | async-start | bytes 8192 | tf_op jit(solution)/shard_map/all_to_all | solution.py:43
  30.7 2.2 %fusion.14 = bf16[8,256]{1,0:T(8,128)(2,1)S(1)} fusion(bf16[4096,1,256]{2,0,1:T(8,128)(2,1)} %param.15, bf16[8,4096]{1,0:T(8,128)(2,1)S(1)} %all_gather.9, f32[4096]{0:T(1024)S(1)} %copy-done.4, f32[8]{0:T(128)S(1)} %add_rsqrt_fusion.2), kind=kOutput, calls=%fused_computation.14 | convolution fusion | flops 16910336 | bytes 2183200 | tf_op jit(solution)/shard_map/dot_general | solution.py:35
  32.8 0.1 copy-done.2
  32.9 0.4 fusion.17
  33.3 0.2 copy-done.3
  33.5 0.4 fusion.11
  34.0 0.6 all_to_all.42
  34.6 0.6 all_to_all.44
  35.2 0.6 all_to_all.40
  35.8 0.5 all-to-all-done.3
  36.2 4.6 %all-to-all-start = ((bf16[4,2,256]{2,1,0:T(2,128)(2,1)}), bf16[4,2,256]{2,1,0:T(2,128)(2,1)S(1)}, u32[]{:S(2)}, u32[]{:S(2)}) async-start(bf16[4,2,256]{2,1,0:T(2,128)(2,1)} %all_to_all.40), calls=%async_computation | async-start | bytes 8192 | tf_op jit(solution)/shard_map/all_to_all | solution.py:40
  40.9 5.6 %all-to-all-done = bf16[4,2,256]{2,1,0:T(2,128)(2,1)S(1)} async-done(((bf16[4,2,256]{2,1,0:T(2,128)(2,1)}), bf16[4,2,256]{2,1,0:T(2,128)(2,1)S(1)}, u32[]{:S(2)}, u32[]{:S(2)}) %all-to-all-start) | async-done | bytes 4128 | tf_op jit(solution)/shard_map/all_to_all | solution.py:40
  46.4 3.2 %all-to-all-start.2 = ((bf16[4,2,256]{2,1,0:T(2,128)(2,1)}), bf16[4,2,256]{2,1,0:T(2,128)(2,1)S(1)}, u32[]{:S(2)}, u32[]{:S(2)}) async-start(bf16[4,2,256]{2,1,0:T(2,128)(2,1)} %all_to_all.44), calls=%async_computation.2 | async-start | bytes 8192 | tf_op jit(solution)/shard_map/all_to_all | solution.py:42
  49.7 5.5 %all-to-all-done.2 = bf16[4,2,256]{2,1,0:T(2,128)(2,1)S(1)} async-done(((bf16[4,2,256]{2,1,0:T(2,128)(2,1)}), bf16[4,2,256]{2,1,0:T(2,128)(2,1)S(1)}, u32[]{:S(2)}, u32[]{:S(2)}) %all-to-all-start.2) | async-done | bytes 4128 | tf_op jit(solution)/shard_map/all_to_all | solution.py:42
  55.2 3.2 %all-to-all-start.1 = ((bf16[4,2,256]{2,1,0:T(2,128)(2,1)}), bf16[4,2,256]{2,1,0:T(2,128)(2,1)S(1)}, u32[]{:S(2)}, u32[]{:S(2)}) async-start(bf16[4,2,256]{2,1,0:T(2,128)(2,1)} %all_to_all.42), calls=%async_computation.1 | async-start | bytes 8192 | tf_op jit(solution)/shard_map/all_to_all | solution.py:41
  58.4 0.0 reduce-scatter.2.cloned.1.call-start
  58.6 5.4 %all-to-all-done.1 = bf16[4,2,256]{2,1,0:T(2,128)(2,1)S(1)} async-done(((bf16[4,2,256]{2,1,0:T(2,128)(2,1)}), bf16[4,2,256]{2,1,0:T(2,128)(2,1)S(1)}, u32[]{:S(2)}, u32[]{:S(2)}) %all-to-all-start.1) | async-done | bytes 4128 | tf_op jit(solution)/shard_map/all_to_all | solution.py:41
  64.0 1.8 %multiply_add_fusion = f32[2,8,128,128]{3,2,1,0:T(8,128)S(1)} fusion(f32[2,8,128,128]{3,2,1,0:T(8,128)} %param.25, f32[2,8,128]{2,1,0:T(8,128)S(1)} %reshape.112, f32[2,8,128]{2,1,0:T(8,128)S(1)} %get-tuple-element.2, f32[2,8,128]{2,1,0:T(8,128)S(1)} %get-tuple-element.3), kind=kLoop, calls=%fused_computation.17 | loop fusion | flops 786432 | bytes 2121728 | tf_op jit(solution)/shard_map/add | solution.py:58
  65.9 1.0 fusion.42
  66.9 0.1 multiply_reduce_fusion
  67.0 0.1 multiply_convert_fusion
  67.1 14.1 %all_gather.10 = bf16[2,8,1024]{2,0,1:T(2,128)(2,1)S(1)} all-gather(bf16[2,1,1024]{2,0,1:T(2,128)(2,1)S(1)} %convert_element_type.111), channel_id=1, replica_groups=mesh['dp'=4,'kv'=4,'tp'=2] {'kv','tp'}, dimensions={1}, use_global_device_ids=true | all-gather | bytes 36864 | tf_op jit(solution)/shard_map/all_gather | solution.py:63
  81.2 0.4 fusion.10
  81.6 14.0 %all_gather.11 = bf16[8,4096]{1,0:T(8,128)(2,1)S(1)} all-gather(bf16[8,512]{1,0:T(8,128)(2,1)S(1)} %fusion.10), channel_id=1, replica_groups=mesh['dp'=4,'kv'=4,'tp'=2] {'kv','tp'}, dimensions={1}, use_global_device_ids=true | all-gather | bytes 73728 | tf_op jit(solution)/shard_map/all_gather | solution.py:70
  95.6 0.1 fusion.27
  95.7 13.5 %fusion.23 = f32[8,4096]{1,0:T(8,128)} fusion(bf16[2048,4096]{1,0:T(8,128)(2,1)} %param.24, bf16[4096,2048]{1,0:T(8,128)(2,1)} %param.23, bf16[8,4096]{1,0:T(8,128)(2,1)S(1)} %all_gather.11, f32[4096]{0:T(1024)S(1)} %copy-done.6, f32[8]{0:T(128)S(1)} %add_rsqrt_fusion.1), kind=kOutput, calls=%fused_computation.18 | convolution fusion | flops 268615680 | bytes 33767456 | tf_op jit(solution)/shard_map/dot_general | solution.py:74
  109.3 28.9 %reduce-scatter.2.cloned.1.call-done = f32[8,512]{1,0:T(8,128)} async-done(((f32[8,4096]{1,0:T(8,128)}), f32[8,512]{1,0:T(8,128)}) %reduce-scatter.2.cloned.1.call-update) | async-done | bytes 16400 | tf_op jit(solution)/shard_map/reduce_scatter | solution.py:75
  138.2 1.3 add_convert_fusion
  (37 shorter events, 0.2 us)
Async XLA Ops:
  7.2 74.0 %copy-start = (bf16[2048,512]{1,0:T(8,128)(2,1)S(1)}, bf16[2048,512]{1,0:T(8,128)(2,1)}, u32[]{:S(2)}) copy-start(bf16[2048,512]{1,0:T(8,128)(2,1)} %param.20) | copy-start | bytes 6291460
  7.2 23.5 %copy-start.4 = (f32[4096]{0:T(1024)S(1)}, f32[4096]{0:T(1024)}, u32[]{:S(2)}) copy-start(f32[4096]{0:T(1024)} %param.21) | copy-start | bytes 49156
  26.0 10.2 %all-to-all-start.3 = ((bf16[4,2,256]{2,1,0:T(2,128)(2,1)}), bf16[4,2,256]{2,1,0:T(2,128)(2,1)S(1)}, u32[]{:S(2)}, u32[]{:S(2)}) async-start(bf16[4,2,256]{2,1,0:T(2,128)(2,1)} %all_to_all.46), calls=%async_computation.3 | async-start | bytes 8192 | tf_op jit(solution)/shard_map/all_to_all | solution.py:43
  30.7 2.2 %copy-start.2 = (bf16[4096,1,256]{2,0,1:T(8,128)(2,1)S(1)}, bf16[4096,1,256]{2,0,1:T(8,128)(2,1)}, u32[]{:S(2)}) copy-start(bf16[4096,1,256]{2,0,1:T(8,128)(2,1)} %param.16) | copy-start | bytes 6291460
  30.7 2.9 %copy-start.3 = (bf16[4096,1,256]{2,0,1:T(8,128)(2,1)S(1)}, bf16[4096,1,256]{2,0,1:T(8,128)(2,1)}, u32[]{:S(2)}) copy-start(bf16[4096,1,256]{2,0,1:T(8,128)(2,1)} %param.14) | copy-start | bytes 6291460
  32.9 1.0 copy-start.7
  33.9 33.0 %copy-start.8 = (f32[128]{0:T(128)S(1)}, f32[128]{0:T(128)}, u32[]{:S(2)}) copy-start(f32[128]{0:T(128)} %param.19) | copy-start | bytes 1540
  33.9 47.3 %copy-start.5 = (bf16[8,512]{1,0:T(8,128)(2,1)S(1)}, bf16[8,512]{1,0:T(8,128)(2,1)}, u32[]{:S(2)}) copy-start(bf16[8,512]{1,0:T(8,128)(2,1)} %param.13) | copy-start | bytes 24580
  36.2 10.2 %all-to-all-start = ((bf16[4,2,256]{2,1,0:T(2,128)(2,1)}), bf16[4,2,256]{2,1,0:T(2,128)(2,1)S(1)}, u32[]{:S(2)}, u32[]{:S(2)}) async-start(bf16[4,2,256]{2,1,0:T(2,128)(2,1)} %all_to_all.40), calls=%async_computation | async-start | bytes 8192 | tf_op jit(solution)/shard_map/all_to_all | solution.py:40
  46.4 8.8 %all-to-all-start.2 = ((bf16[4,2,256]{2,1,0:T(2,128)(2,1)}), bf16[4,2,256]{2,1,0:T(2,128)(2,1)S(1)}, u32[]{:S(2)}, u32[]{:S(2)}) async-start(bf16[4,2,256]{2,1,0:T(2,128)(2,1)} %all_to_all.44), calls=%async_computation.2 | async-start | bytes 8192 | tf_op jit(solution)/shard_map/all_to_all | solution.py:42
  55.2 8.8 %all-to-all-start.1 = ((bf16[4,2,256]{2,1,0:T(2,128)(2,1)}), bf16[4,2,256]{2,1,0:T(2,128)(2,1)S(1)}, u32[]{:S(2)}, u32[]{:S(2)}) async-start(bf16[4,2,256]{2,1,0:T(2,128)(2,1)} %all_to_all.42), calls=%async_computation.1 | async-start | bytes 8192 | tf_op jit(solution)/shard_map/all_to_all | solution.py:41
  58.4 79.8 %reduce-scatter.2.cloned.1.call-start = ((), (), s32[]{:S(2)}) async-start(), calls=%async_computation.5 | async-start | bytes 147456 | tf_op jit(solution)/shard_map/reduce_scatter | solution.py:75
  65.9 43.4 %copy-start.1 = (f32[2,8,128,128]{3,2,1,0:T(8,128)}, f32[2,8,128,128]{3,2,1,0:T(8,128)S(1)}, u32[]{:S(2)}) copy-start(f32[2,8,128,128]{3,2,1,0:T(8,128)S(1)} %multiply_add_fusion) | copy-start | bytes 3145732
  65.9 29.9 %copy-start.6 = (f32[4096]{0:T(1024)S(1)}, f32[4096]{0:T(1024)}, u32[]{:S(2)}) copy-start(f32[4096]{0:T(1024)} %param.22) | copy-start | bytes 49156
Sparse Core Ops, SparseCore 0:
  109.4 28.7 reduce-scatter.1
where the time goes:
time: 147 us; the launch traced here: 146 us
  waiting for transfers between devices  45.9 us (31%)
  blocking collectives  44.1 us (30%)
  matrix products  19.9 us (14%)
  starting transfers between devices  15.7 us (11%)
  between operations  14.2 us (10%)
  other arithmetic  3.68 us (3%)
  local copies, waits for them, and re-layouts  2.83 us (2%)
    reduce_scatter x1, waiting for transfers between devices, per_device(): lax.psum_scatter(partial_terms, ('kv', 'tp'), scatter_dimension=1, tiled=...  28.9 us
    all_gather x1, blocking collectives, per_device(): full_rows = lax.all_gather(tokens, ('kv', 'tp'), axis=1, tiled=True)  16 us
    all_gather x1, blocking collectives, per_device(): gathered = lax.all_gather(branch, ('kv', 'tp'), axis=1, tiled=True)  14.1 us
    all_gather x1, blocking collectives, per_device(): whole_rows = lax.all_gather(residual_one, ('kv', 'tp'), axis=1, tiled=True)  14 us
    dot_general x1, matrix products, per_device(): partial_terms = jnp.dot(hidden, w_down, preferred_element_type=jnp.float32)  13.5 us
    all_to_all x1, waiting for transfers between devices, per_device(): lax.all_to_all(project(w_query), 'kv', split_axis=0, concat_axis=1, tiled...  5.57 us
    all_to_all x1, waiting for transfers between devices, per_device(): lax.all_to_all(project(w_input), 'kv', split_axis=0, concat_axis=1, tiled...  5.53 us
    all_to_all x1, waiting for transfers between devices, per_device(): lax.all_to_all(project(w_forget), 'kv', split_axis=0, concat_axis=1, tile...  5.41 us
  transfers between devices with their start and end apart: 5, of which 5 were waited for; matrix products, arithmetic and copies ran while one was open for 2% of the time, Pallas kernels for 0%

commit v1 on v0

--- a/solution.py
+++ b/solution.py
@@ -25,6 +25,18 @@
     w_down,
     state,
 ):
+
+    def change_floor(local_values):
+        return jnp.concatenate(
+            lax.all_to_all(
+                jnp.stack(jnp.split(local_values, lax.psum(1, axis_name="kv"), axis=0)),
+                axis_name="kv",
+                split_axis=0,
+                concat_axis=0,
+            ),
+            axis=1,
+        )
+
     group_kv = lax.axis_size("kv")
     group_tp = lax.axis_size("tp")
     tokens_f = tokens.astype(jnp.float32)
@@ -39,7 +51,7 @@
     query_raw, forget_raw, input_raw, gate_raw = (
         lax.all_to_all(project(w_query), "kv", split_axis=0, concat_axis=1, tiled=True),
         lax.all_to_all(project(w_forget), "kv", split_axis=0, concat_axis=1, tiled=True),
-        lax.all_to_all(project(w_input), "kv", split_axis=0, concat_axis=1, tiled=True),
+        change_floor(project(w_input)),
         lax.all_to_all(project(w_output_gate), "kv", split_axis=0, concat_axis=1, tiled=True),
     )
     seq_local = state.shape[0]

time: 147 us -> 147 us (level)
  transfers between devices with their start and end apart: 5 -> 5, of which waited for: 5 -> 5; matrix products, arithmetic and copies ran while one was open for 2% -> 3% of each run, Pallas kernels for 0% -> 0%
where the time goes in v1:
time: 147 us; the launch traced here: 146 us
  waiting for transfers between devices  45.9 us (31%)
  blocking collectives  44.1 us (30%)
  matrix products  19.9 us (14%)
  starting transfers between devices  15.7 us (11%)
  between operations  14.2 us (10%)
  other arithmetic  4.29 us (3%)
  local copies, waits for them, and re-layouts  2.2 us (1%)
    reduce_scatter x1, waiting for transfers between devices, per_device(): lax.psum_scatter(partial_terms, ('kv', 'tp'), scatter_dimension=1, tiled=...  28.9 us
    all_gather x1, blocking collectives, per_device(): full_rows = lax.all_gather(tokens, ('kv', 'tp'), axis=1, tiled=True)  16 us
    all_gather x1, blocking collectives, per_device(): gathered = lax.all_gather(branch, ('kv', 'tp'), axis=1, tiled=True)  14.1 us
    all_gather x1, blocking collectives, per_device(): whole_rows = lax.all_gather(residual_one, ('kv', 'tp'), axis=1, tiled=True)  14 us
    dot_general x1, matrix products, per_device(): partial_terms = jnp.dot(hidden, w_down, preferred_element_type=jnp.float32)  13.5 us
    all_to_all x1, waiting for transfers between devices, per_device(): lax.all_to_all(project(w_query), 'kv', split_axis=0, concat_axis=1, tiled...  5.57 us
    all_to_all x1, waiting for transfers between devices, change_floor(): lax.all_to_all(jnp.stack(jnp.split(local_values, lax.psum(1, axis_name='k...  5.53 us
    all_to_all x1, waiting for transfers between devices, per_device(): lax.all_to_all(project(w_forget), 'kv', split_axis=0, concat_axis=1, tile...  5.41 us
  transfers between devices with their start and end apart: 5, of which 5 were waited for; matrix products, arithmetic and copies ran while one was open for 3% of the time, Pallas kernels for 0%

profile of v1, /device:TPU:0, one launch (start us, length us, event | category | flops | bytes accessed | tf_op | source)
XLA Modules:
  0.0 146.4 jit_solution(452440304205924939)
XLA Ops:
  7.2 16.0 %all_gather.9 = bf16[8,4096]{1,0:T(8,128)(2,1)S(1)} all-gather(bf16[8,512]{1,0:T(8,128)(2,1)} %param.13), channel_id=1, replica_groups=mesh['dp'=4,'kv'=4,'tp'=2] {'kv','tp'}, dimensions={1}, use_global_device_ids=true | all-gather | bytes 73728 | tf_op jit(solution)/shard_map/all_gather | solution.py:43
  23.2 0.1 fusion.24
  23.4 2.0 %fusion.20 = bf16[8,256]{1,0:T(8,128)(2,1)S(1)} fusion(bf16[4096,1,256]{2,0,1:T(8,128)(2,1)} %param.17, bf16[8,4096]{1,0:T(8,128)(2,1)S(1)} %all_gather.9, f32[4096]{0:T(1024)} %param.21, f32[8]{0:T(128)S(1)} %add_rsqrt_fusion.2), kind=kOutput, calls=%fused_computation.16 | convolution fusion | flops 16910336 | bytes 2183200 | tf_op jit(solution)/shard_map/dot_general | solution.py:47
  25.4 0.6 all_to_all.38
  26.0 4.6 %all-to-all-start.3 = ((bf16[4,2,256]{2,1,0:T(2,128)(2,1)}), bf16[4,2,256]{2,1,0:T(2,128)(2,1)S(1)}, u32[]{:S(2)}, u32[]{:S(2)}) async-start(bf16[4,2,256]{2,1,0:T(2,128)(2,1)} %all_to_all.38), calls=%async_computation.3 | async-start | bytes 8192 | tf_op jit(solution)/shard_map/all_to_all | solution.py:55
  30.7 2.2 %fusion.14 = bf16[8,256]{1,0:T(8,128)(2,1)S(1)} fusion(bf16[4096,1,256]{2,0,1:T(8,128)(2,1)} %param.15, bf16[8,4096]{1,0:T(8,128)(2,1)S(1)} %all_gather.9, f32[4096]{0:T(1024)S(1)} %copy-done.4, f32[8]{0:T(128)S(1)} %add_rsqrt_fusion.2), kind=kOutput, calls=%fused_computation.14 | convolution fusion | flops 16910336 | bytes 2183200 | tf_op jit(solution)/shard_map/dot_general | solution.py:47
  32.9 0.0 copy-done.2
  32.9 0.4 fusion.17
  33.3 0.2 copy-done.3
  33.5 0.4 fusion.11
  34.0 0.6 pad_maximum_fusion
  34.6 0.6 all_to_all.35
  35.2 0.6 all_to_all.33
  35.8 0.5 all-to-all-done.3
  36.3 4.6 %all-to-all-start = ((bf16[4,2,256]{2,1,0:T(2,128)(2,1)}), bf16[4,2,256]{2,1,0:T(2,128)(2,1)S(1)}, u32[]{:S(2)}, u32[]{:S(2)}) async-start(bf16[4,2,256]{2,1,0:T(2,128)(2,1)} %all_to_all.33), calls=%async_computation | async-start | bytes 8192 | tf_op jit(solution)/shard_map/all_to_all | solution.py:52
  40.9 5.6 %all-to-all-done = bf16[4,2,256]{2,1,0:T(2,128)(2,1)S(1)} async-done(((bf16[4,2,256]{2,1,0:T(2,128)(2,1)}), bf16[4,2,256]{2,1,0:T(2,128)(2,1)S(1)}, u32[]{:S(2)}, u32[]{:S(2)}) %all-to-all-start) | async-done | bytes 4128 | tf_op jit(solution)/shard_map/all_to_all | solution.py:52
  46.4 3.2 %all-to-all-start.2 = ((bf16[4,2,256]{2,1,0:T(2,128)(2,1)}), bf16[4,2,256]{2,1,0:T(2,128)(2,1)S(1)}, u32[]{:S(2)}, u32[]{:S(2)}) async-start(bf16[4,2,256]{2,1,0:T(2,128)(2,1)} %pad_maximum_fusion), calls=%async_computation.2 | async-start | bytes 8192 | tf_op jit(solution)/shard_map/all_to_all | solution.py:31
  49.7 5.5 %all-to-all-done.2 = bf16[4,2,256]{2,1,0:T(2,128)(2,1)S(1)} async-done(((bf16[4,2,256]{2,1,0:T(2,128)(2,1)}), bf16[4,2,256]{2,1,0:T(2,128)(2,1)S(1)}, u32[]{:S(2)}, u32[]{:S(2)}) %all-to-all-start.2) | async-done | bytes 4128 | tf_op jit(solution)/shard_map/all_to_all | solution.py:31
  55.2 3.2 %all-to-all-start.1 = ((bf16[4,2,256]{2,1,0:T(2,128)(2,1)}), bf16[4,2,256]{2,1,0:T(2,128)(2,1)S(1)}, u32[]{:S(2)}, u32[]{:S(2)}) async-start(bf16[4,2,256]{2,1,0:T(2,128)(2,1)} %all_to_all.35), calls=%async_computation.1 | async-start | bytes 8192 | tf_op jit(solution)/shard_map/all_to_all | solution.py:53
  58.4 0.0 reduce-scatter.2.cloned.1.call-start
  58.6 5.4 %all-to-all-done.1 = bf16[4,2,256]{2,1,0:T(2,128)(2,1)S(1)} async-done(((bf16[4,2,256]{2,1,0:T(2,128)(2,1)}), bf16[4,2,256]{2,1,0:T(2,128)(2,1)S(1)}, u32[]{:S(2)}, u32[]{:S(2)}) %all-to-all-start.1) | async-done | bytes 4128 | tf_op jit(solution)/shard_map/all_to_all | solution.py:53
  64.0 1.8 %multiply_add_fusion = f32[2,8,128,128]{3,2,1,0:T(8,128)S(1)} fusion(f32[2,8,128,128]{3,2,1,0:T(8,128)} %param.25, f32[2,8,128]{2,1,0:T(8,128)S(1)} %reshape.111, f32[2,8,128]{2,1,0:T(8,128)S(1)} %get-tuple-element.2, f32[2,8,128]{2,1,0:T(8,128)S(1)} %get-tuple-element.3), kind=kLoop, calls=%fused_computation.17 | loop fusion | flops 786432 | bytes 2121728 | tf_op jit(solution)/shard_map/add | solution.py:70
  65.9 1.0 fusion.42
  66.9 0.1 multiply_reduce_fusion
  67.0 0.1 multiply_convert_fusion
  67.1 14.1 %all_gather.10 = bf16[2,8,1024]{2,0,1:T(2,128)(2,1)S(1)} all-gather(bf16[2,1,1024]{2,0,1:T(2,128)(2,1)S(1)} %convert_element_type.111), channel_id=1, replica_groups=mesh['dp'=4,'kv'=4,'tp'=2] {'kv','tp'}, dimensions={1}, use_global_device_ids=true | all-gather | bytes 36864 | tf_op jit(solution)/shard_map/all_gather | solution.py:75
  81.2 0.4 fusion.10
  81.6 14.0 %all_gather.11 = bf16[8,4096]{1,0:T(8,128)(2,1)S(1)} all-gather(bf16[8,512]{1,0:T(8,128)(2,1)S(1)} %fusion.10), channel_id=1, replica_groups=mesh['dp'=4,'kv'=4,'tp'=2] {'kv','tp'}, dimensions={1}, use_global_device_ids=true | all-gather | bytes 73728 | tf_op jit(solution)/shard_map/all_gather | solution.py:82
  95.6 0.1 fusion.27
  95.8 13.5 %fusion.23 = f32[8,4096]{1,0:T(8,128)} fusion(bf16[2048,4096]{1,0:T(8,128)(2,1)} %param.24, bf16[4096,2048]{1,0:T(8,128)(2,1)} %param.23, bf16[8,4096]{1,0:T(8,128)(2,1)S(1)} %all_gather.11, f32[4096]{0:T(1024)S(1)} %copy-done.6, f32[8]{0:T(128)S(1)} %add_rsqrt_fusion.1), kind=kOutput, calls=%fused_computation.18 | convolution fusion | flops 268615680 | bytes 33767456 | tf_op jit(solution)/shard_map/dot_general | solution.py:86
  109.3 28.9 %reduce-scatter.2.cloned.1.call-done = f32[8,512]{1,0:T(8,128)} async-done(((f32[8,4096]{1,0:T(8,128)}), f32[8,512]{1,0:T(8,128)}) %reduce-scatter.2.cloned.1.call-update) | async-done | bytes 16400 | tf_op jit(solution)/shard_map/reduce_scatter | solution.py:87
  138.2 1.3 add_convert_fusion
  (38 shorter events, 0.2 us)
Async XLA Ops:
  7.2 74.0 %copy-start = (bf16[2048,512]{1,0:T(8,128)(2,1)S(1)}, bf16[2048,512]{1,0:T(8,128)(2,1)}, u32[]{:S(2)}) copy-start(bf16[2048,512]{1,0:T(8,128)(2,1)} %param.20) | copy-start | bytes 6291460
  7.2 23.5 %copy-start.4 = (f32[4096]{0:T(1024)S(1)}, f32[4096]{0:T(1024)}, u32[]{:S(2)}) copy-start(f32[4096]{0:T(1024)} %param.21) | copy-start | bytes 49156
  7.2 23.5 %copy-start.7 = (f32[1024]{0:T(1024)S(1)}, f32[1024]{0:T(1024)}, u32[]{:S(2)}) copy-start(f32[1024]{0:T(1024)} %param.18) | copy-start | bytes 12292
  26.0 10.2 %all-to-all-start.3 = ((bf16[4,2,256]{2,1,0:T(2,128)(2,1)}), bf16[4,2,256]{2,1,0:T(2,128)(2,1)S(1)}, u32[]{:S(2)}, u32[]{:S(2)}) async-start(bf16[4,2,256]{2,1,0:T(2,128)(2,1)} %all_to_all.38), calls=%async_computation.3 | async-start | bytes 8192 | tf_op jit(solution)/shard_map/all_to_all | solution.py:55
  30.7 2.2 %copy-start.2 = (bf16[4096,1,256]{2,0,1:T(8,128)(2,1)S(1)}, bf16[4096,1,256]{2,0,1:T(8,128)(2,1)}, u32[]{:S(2)}) copy-start(bf16[4096,1,256]{2,0,1:T(8,128)(2,1)} %param.16) | copy-start | bytes 6291460
  30.7 2.8 %copy-start.3 = (bf16[4096,1,256]{2,0,1:T(8,128)(2,1)S(1)}, bf16[4096,1,256]{2,0,1:T(8,128)(2,1)}, u32[]{:S(2)}) copy-start(bf16[4096,1,256]{2,0,1:T(8,128)(2,1)} %param.14) | copy-start | bytes 6291460
  34.0 33.0 %copy-start.8 = (f32[128]{0:T(128)S(1)}, f32[128]{0:T(128)}, u32[]{:S(2)}) copy-start(f32[128]{0:T(128)} %param.19) | copy-start | bytes 1540
  34.0 47.3 %copy-start.5 = (bf16[8,512]{1,0:T(8,128)(2,1)S(1)}, bf16[8,512]{1,0:T(8,128)(2,1)}, u32[]{:S(2)}) copy-start(bf16[8,512]{1,0:T(8,128)(2,1)} %param.13) | copy-start | bytes 24580
  36.3 10.2 %all-to-all-start = ((bf16[4,2,256]{2,1,0:T(2,128)(2,1)}), bf16[4,2,256]{2,1,0:T(2,128)(2,1)S(1)}, u32[]{:S(2)}, u32[]{:S(2)}) async-start(bf16[4,2,256]{2,1,0:T(2,128)(2,1)} %all_to_all.33), calls=%async_computation | async-start | bytes 8192 | tf_op jit(solution)/shard_map/all_to_all | solution.py:52
  46.4 8.8 %all-to-all-start.2 = ((bf16[4,2,256]{2,1,0:T(2,128)(2,1)}), bf16[4,2,256]{2,1,0:T(2,128)(2,1)S(1)}, u32[]{:S(2)}, u32[]{:S(2)}) async-start(bf16[4,2,256]{2,1,0:T(2,128)(2,1)} %pad_maximum_fusion), calls=%async_computation.2 | async-start | bytes 8192 | tf_op jit(solution)/shard_map/all_to_all | solution.py:31
  55.2 8.8 %all-to-all-start.1 = ((bf16[4,2,256]{2,1,0:T(2,128)(2,1)}), bf16[4,2,256]{2,1,0:T(2,128)(2,1)S(1)}, u32[]{:S(2)}, u32[]{:S(2)}) async-start(bf16[4,2,256]{2,1,0:T(2,128)(2,1)} %all_to_all.35), calls=%async_computation.1 | async-start | bytes 8192 | tf_op jit(solution)/shard_map/all_to_all | solution.py:53
  58.4 79.8 %reduce-scatter.2.cloned.1.call-start = ((), (), s32[]{:S(2)}) async-start(), calls=%async_computation.5 | async-start | bytes 147456 | tf_op jit(solution)/shard_map/reduce_scatter | solution.py:87
  65.9 43.4 %copy-start.1 = (f32[2,8,128,128]{3,2,1,0:T(8,128)}, f32[2,8,128,128]{3,2,1,0:T(8,128)S(1)}, u32[]{:S(2)}) copy-start(f32[2,8,128,128]{3,2,1,0:T(8,128)S(1)} %multiply_add_fusion) | copy-start | bytes 3145732
  65.9 29.9 %copy-start.6 = (f32[4096]{0:T(1024)S(1)}, f32[4096]{0:T(1024)}, u32[]{:S(2)}) copy-start(f32[4096]{0:T(1024)} %param.22) | copy-start | bytes 49156
Sparse Core Ops, SparseCore 0:
  109.4 28.7 reduce-scatter.1
